TPU v7x, 32 devices: a whole 2x2x4 slice. The times are simulated.
32 devices in a mesh: ep: 8 (over z, x), tp: 4 (over y, core).
Axes of the slice: x: 2, y: 2, z: 4, core: 2. Of those that a mesh axis runs over, the one named last changes fastest.
Arguments:
- tokens: bfloat16 [192, 3072], P('ep'), may hold values from -6 to 6
- norm_gain: float32 [3072], replicated, may hold values from 0.1 to 1.9
- routing: int32 [192, 4], P('ep'), may hold values from 0 to 7, all different within a row; in each aligned block of 24 rows (0 to 23, 24 to 47, ...) at most 13 rows name the same one
- route_weight: float32 [192, 4], P('ep'), may hold values from 0.05 to 1
- w_gate: bfloat16 [8, 3072, 3072], P('ep', None, 'tp'), may hold values from -0.3125 to 0.3125
- w_up: bfloat16 [8, 3072, 3072], P('ep', None, 'tp'), may hold values from -0.3125 to 0.3125
- w_down: bfloat16 [8, 3072, 3072], P('ep', 'tp'), may hold values from -0.01953125 to 0.01953125
Outputs:
- mixed: bfloat16 [192, 3072], P('ep', 'tp')
Inputs may be any that keep to these rules, and one draw needn't show every extreme that they name: `routing`: each row names 4 different experts. Within the rows of one device (aligned blocks of 24 rows) no expert is named by more than 13 rows, a bound that some block reaches.
All inputs are finite; a program needn't handle non-finite values.
Results may differ from a plain program's by a relative error of at most 0.019.
Values may be sent and summed in bfloat16 or wider, within the bound.
No kernel may reach another device: no remote copies, remote signals or barrier semaphores. Data moves between devices by JAX's collectives and lax.ppermute only.
A program may use at most 64 MiB of HBM per device.

v0:
```python
import jax
import jax.numpy as jnp
from jax import lax
from jax.sharding import PartitionSpec as P

NORM_EPS = 1e-06
CLAMP_LIMIT = 7.0
SIGMOID_SCALE = 1.702


def slot_index(route_rows, expert_total, capacity):
    flat_ids = route_rows.reshape(-1)
    one_hot = (flat_ids[:, None] == jnp.arange(expert_total, dtype=jnp.int32)[None, :]).astype(
        jnp.int32
    )
    before = jnp.cumsum(one_hot, axis=0) - one_hot
    ranked = jnp.sum(before * one_hot, axis=1)
    return flat_ids * capacity + ranked


def local(tokens, norm_gain, routing, route_weight, w_gate, w_up, w_down):
    tok_count = tokens.shape[0]
    width = tokens.shape[1]
    top_count = routing.shape[1]
    expert_total = lax.axis_size("ep") * w_gate.shape[0]
    capacity = max(2, tok_count * top_count // expert_total + 1)
    slice_width = width // lax.axis_size("tp")
    values = tokens.astype(jnp.float32)
    scaled = values * lax.rsqrt(jnp.mean(values * values, axis=-1, keepdims=True) + NORM_EPS)
    normal = (scaled * norm_gain).astype(jnp.bfloat16)
    dest = slot_index(routing, expert_total, capacity)
    slot_ids = jnp.arange(expert_total * capacity, dtype=jnp.int32)
    select = jnp.sum(dest.reshape(1, tok_count, top_count) == slot_ids[:, None, None], axis=2)
    sending = jnp.dot(
        select.astype(jnp.bfloat16), normal, preferred_element_type=jnp.float32
    ).astype(jnp.bfloat16)
    gate_mat = w_gate[0]
    up_mat = w_up[0]
    down_mat = w_down[0]
    own_share = lax.dynamic_slice_in_dim(
        sending, lax.axis_index("tp") * slice_width, slice_width, 1
    )
    arrived = lax.all_to_all(own_share, "ep", split_axis=0, concat_axis=0, tiled=True)
    pieces = lax.all_gather(arrived, "tp", axis=1, tiled=True)
    gate_pre = jnp.dot(pieces, gate_mat, preferred_element_type=jnp.float32)
    up_pre = jnp.dot(pieces, up_mat, preferred_element_type=jnp.float32)
    gated = jnp.minimum(gate_pre, CLAMP_LIMIT)
    upper = jnp.clip(up_pre, -CLAMP_LIMIT, CLAMP_LIMIT)
    hidden = ((upper + 1.0) * gated * jax.nn.sigmoid(SIGMOID_SCALE * gated)).astype(jnp.bfloat16)
    summed = lax.psum_scatter(
        lax.dot_general(
            down_mat, hidden, (((0,), (1,)), ((), ())), preferred_element_type=jnp.float32
        ).astype(jnp.bfloat16),
        "tp",
        scatter_dimension=0,
        tiled=True,
    )
    back = lax.all_to_all(summed, "ep", split_axis=1, concat_axis=1, tiled=True)
    picked = back[:, dest].reshape(slice_width, tok_count, top_count)
    mixed = jnp.sum(picked.astype(jnp.float32) * route_weight[None, :, :], axis=2)
    return mixed.T.astype(jnp.bfloat16)


def solution(mesh):
    placed = (
        P("ep", None),
        P(),
        P("ep", None),
        P("ep", None),
        P("ep", None, "tp"),
        P("ep", None, "tp"),
        P("ep", "tp", None),
    )
    return jax.shard_map(
        local, mesh=mesh, in_specs=placed, out_specs=P("ep", "tp"), check_vma=False
    )
```

profile of v0, /device:TPU:0, one launch (start us, length us, event | category | flops | bytes accessed | tf_op | source)
XLA Modules:
  0.0 87.3 jit_solution(828306079801427838)
XLA Ops:
  6.5 0.8 copy.14
  7.3 0.1 eq.28
  7.4 0.1 fusion.48
  7.5 0.1 reduce_window_sum.11
  7.6 0.2 select_reduce_fusion
  7.8 0.1 reduce_sum.41
  7.9 0.1 copy.16
  8.0 0.1 convert_reduce_fusion
  8.1 1.0 %fusion.37 = f32[24]{0:T(128)S(1)} fusion(bf16[24,3072]{1,0:T(8,128)(2,1)} %param.7), kind=kLoop, calls=%fused_computation.23 | loop fusion | flops 221160 | bytes 147552 | tf_op jit(solution)/shard_map/reduce_sum | solution.py:29
  9.2 1.3 %fusion.44 = bf16[104,3072]{1,0:T(8,128)(2,1)S(1)} fusion(bf16[24,3072]{1,0:T(8,128)(2,1)} %param.7, f32[3072]{0:T(1024)} %param.8, f32[24]{0:T(128)S(1)} %add_rsqrt_fusion, s32[104,24]{0,1:T(8,128)S(1)} %convert_reduce_fusion), kind=kOutput, calls=%fused_computation.32 | convolution fusion | flops 15632832 | bytes 808800 | tf_op jit(solution)/shard_map/dot_general | solution.py:34
  10.6 15.0 %all_to_all.24 = bf16[8,13,768]{2,1,0:T(8,128)(2,1)S(1)} all-to-all(bf16[8,13,768]{2,1,0:T(8,128)(2,1)S(1)} %all_to_all.16), channel_id=1, replica_groups=mesh['ep'=8,'tp'=4] {'ep'}, dimensions={0} | all-to-all | bytes 319488 | tf_op jit(solution)/shard_map/all_to_all | solution.py:43
  25.6 0.1 all_to_all.18
  25.7 7.8 %all_gather.3 = bf16[104,3072]{1,0:T(8,128)(2,1)S(1)} all-gather(bf16[104,768]{1,0:T(8,128)(2,1)S(1)} %all_to_all.18), channel_id=1, replica_groups=mesh['ep'=8,'tp'=4] {'tp'}, dimensions={1}, use_global_device_ids=true | all-gather | bytes 798720 | tf_op jit(solution)/shard_map/all_gather | solution.py:44
  33.5 3.2 %fusion.12 = f32[104,768]{1,0:T(8,128)S(1)} fusion(bf16[104,3072]{1,0:T(8,128)(2,1)S(1)} %all_gather.3, bf16[1,3072,768]{2,1,0:T(8,128)(2,1)} %param.11), kind=kOutput, calls=%fused_computation.9 | convolution fusion | flops 490813440 | bytes 5677056 | tf_op jit(solution)/shard_map/dot_general | solution.py:45
  36.7 6.5 %fusion.9 = bf16[3072,104]{0,1:T(8,128)(2,1)} fusion(bf16[1,768,3072]{2,1,0:T(8,128)(2,1)} %param.13, f32[104,768]{1,0:T(8,128)S(1)} %fusion.12, bf16[104,3072]{1,0:T(8,128)(2,1)S(1)} %all_gather.3, bf16[1,3072,768]{2,1,0:T(8,128)(2,1)} %param.12), kind=kOutput, calls=%fused_computation.8 | convolution fusion | flops 982505472 | bytes 11034624 | tf_op jit(solution)/shard_map/dot_general | solution.py:51
  43.2 0.1 mul.76
  43.4 0.1 copy.17
  43.4 20.2 %reduce-scatter.2.cloned.1.call-done = bf16[768,104]{0,1:T(8,128)(2,1)} async-done(((bf16[3072,104]{0,1:T(8,128)(2,1)}), bf16[768,104]{0,1:T(8,128)(2,1)}) %reduce-scatter.2.cloned.1.call-update) | async-done | bytes 159760 | tf_op jit(solution)/shard_map/reduce_scatter | solution.py:50
  63.7 1.6 %all_to_all.19 = bf16[768,8,13]{0,2,1:T(8,128)(2,1)} reshape(bf16[768,104]{0,1:T(8,128)(2,1)} %reduce-scatter.2.cloned.1.call-done) | data formatting | bytes 319488 | tf_op jit(solution)/shard_map/all_to_all | solution.py:58
  65.3 5.5 %all-to-all-start.1 = ((bf16[768,8,13]{0,2,1:T(8,128)(2,1)}), bf16[768,8,13]{0,2,1:T(8,128)(2,1)S(1)}, u32[]{:S(2)}, u32[]{:S(2)}) async-start(bf16[768,8,13]{0,2,1:T(8,128)(2,1)} %all_to_all.19), calls=%async_computation.2 | async-start | bytes 393216 | tf_op jit(solution)/shard_map/all_to_all | solution.py:58
  70.8 7.8 %all-to-all-done.1 = bf16[768,8,13]{0,2,1:T(8,128)(2,1)S(1)} async-done(((bf16[768,8,13]{0,2,1:T(8,128)(2,1)}), bf16[768,8,13]{0,2,1:T(8,128)(2,1)S(1)}, u32[]{:S(2)}, u32[]{:S(2)}) %all-to-all-start.1) | async-done | bytes 159776 | tf_op jit(solution)/shard_map/all_to_all | solution.py:58
  78.7 0.8 gather_fusion
  79.5 0.1 reshape.54
  79.6 0.9 multiply_reduce_fusion
  (12 shorter events, 0.2 us)
Async XLA Ops:
  6.5 57.1 %reduce-scatter.2.cloned.1.call-start = ((), (), s32[]{:S(2)}) async-start(), calls=%async_computation.3 | async-start | bytes 798720 | tf_op jit(solution)/shard_map/reduce_scatter | solution.py:50
  36.7 6.7 %copy-start = (f32[24,4]{0,1:T(4,128)S(1)}, f32[24,4]{0,1:T(4,128)}, u32[]{:S(2)}) copy-start(f32[24,4]{0,1:T(4,128)} %param.10) | copy-start | bytes 1156
  65.3 13.3 %all-to-all-start.1 = ((bf16[768,8,13]{0,2,1:T(8,128)(2,1)}), bf16[768,8,13]{0,2,1:T(8,128)(2,1)S(1)}, u32[]{:S(2)}, u32[]{:S(2)}) async-start(bf16[768,8,13]{0,2,1:T(8,128)(2,1)} %all_to_all.19), calls=%async_computation.2 | async-start | bytes 393216 | tf_op jit(solution)/shard_map/all_to_all | solution.py:58
Sparse Core Ops, SparseCore 0:
  43.4 20.2 reduce-scatter.1
where the time goes:
time: 87.7 us; the launch traced here: 87.3 us
  waiting for transfers between devices  28 us (32%)
  blocking collectives  22.9 us (26%)
  between operations  13.5 us (15%)
  matrix products  11 us (13%)
  starting transfers between devices  5.5 us (6%)
  local copies, waits for them, and re-layouts  3.96 us (5%)
  other arithmetic  2.44 us (3%)
    reduce_scatter x1, waiting for transfers between devices, local(): lax.psum_scatter(lax.dot_general(down_mat, hidden, (((0,), (1,)), ((), ()...  20.2 us
    all_to_all x1, blocking collectives, local(): lax.all_to_all(own_share, 'ep', split_axis=0, concat_axis=0, tiled=True)  15 us
    all_gather x1, blocking collectives, local(): pieces = lax.all_gather(arrived, 'tp', axis=1, tiled=True)  7.82 us
    all_to_all x1, waiting for transfers between devices, local(): back = lax.all_to_all(summed, 'ep', split_axis=1, concat_axis=1, tiled=True)  7.77 us
    dot_general x1, matrix products, local(): lax.dot_general(down_mat, hidden, (((0,), (1,)), ((), ())), preferred_ele...  6.54 us
    all_to_all x1, starting transfers between devices, local(): back = lax.all_to_all(summed, 'ep', split_axis=1, concat_axis=1, tiled=True)  5.5 us
    dot_general x1, matrix products, local(): gate_pre = jnp.dot(pieces, gate_mat, preferred_element_type=jnp.float32)  3.18 us
  transfers between devices with their start and end apart: 2, of which 2 were waited for; matrix products, arithmetic and copies ran while one was open for 0% of the time, Pallas kernels for 0%

commit v1 on v0

--- a/solution.py
+++ b/solution.py
@@ -1,3 +1,4 @@
+import functools
 import jax
 import jax.numpy as jnp
 from jax import lax
@@ -6,6 +7,25 @@
 NORM_EPS = 1e-06
 CLAMP_LIMIT = 7.0
 SIGMOID_SCALE = 1.702
+
+
+def slabs_prepare(original, d_out):
+    amount_of = lax.axis_size("tp")
+    side_arr = sorted(((tick, (tick + 1) % amount_of) for tick in range(amount_of)))
+    right_arr = original
+    queue = [right_arr]
+    num = 1
+    while num < amount_of:
+        right_arr = lax.ppermute(right_arr, "tp", side_arr)
+        queue.insert(0, right_arr)
+        num += 1
+    carry_out = jnp.concatenate(queue, axis=d_out)
+    x_next = lax.axis_index("tp")
+    field_out = x_next + 1
+    return jnp.roll(carry_out, field_out * original.shape[d_out], axis=d_out)
+
+
+answer_pipes_on_mesh = functools.partial(slabs_prepare, d_out=1)
 
 
 def slot_index(route_rows, expert_total, capacity):
@@ -41,7 +61,7 @@
         sending, lax.axis_index("tp") * slice_width, slice_width, 1
     )
     arrived = lax.all_to_all(own_share, "ep", split_axis=0, concat_axis=0, tiled=True)
-    pieces = lax.all_gather(arrived, "tp", axis=1, tiled=True)
+    pieces = answer_pipes_on_mesh(arrived)
     gate_pre = jnp.dot(pieces, gate_mat, preferred_element_type=jnp.float32)
     up_pre = jnp.dot(pieces, up_mat, preferred_element_type=jnp.float32)
     gated = jnp.minimum(gate_pre, CLAMP_LIMIT)

time: 87.7 us -> 95 us (1.083)
  waiting for transfers between devices: 28 us -> 42.7 us
  blocking collectives: 22.9 us -> 15 us
    ppermute x0 -> x3, waiting for transfers between devices: none -> 14.1 us  [slabs_prepare(): right_arr = lax.ppermute(right_arr, 'tp', side_arr)]
    all_gather x1 -> x0, blocking collectives: 7.82 us -> none  [local(): pieces = lax.all_gather(arrived, 'tp', axis=1, tiled=True)]
  transfers between devices with their start and end apart: 2 -> 5, of which waited for: 2 -> 5; matrix products, arithmetic and copies ran while one was open for 0% -> 0% of each run, Pallas kernels for 0% -> 0%
where the time goes in v1:
time: 95 us; the launch traced here: 94.6 us
  waiting for transfers between devices  42.7 us (45%)
  blocking collectives  15 us (16%)
  between operations  13.6 us (14%)
  matrix products  11.2 us (12%)
  starting transfers between devices  5.59 us (6%)
  local copies, waits for them, and re-layouts  4.07 us (4%)
  other arithmetic  2.44 us (3%)
    reduce_scatter x1, waiting for transfers between devices, local(): lax.psum_scatter(lax.dot_general(down_mat, hidden, (((0,), (1,)), ((), ()...  20.9 us
    all_to_all x1, blocking collectives, local(): lax.all_to_all(own_share, 'ep', split_axis=0, concat_axis=0, tiled=True)  15 us
    ppermute x3, waiting for transfers between devices, slabs_prepare(): right_arr = lax.ppermute(right_arr, 'tp', side_arr)  14.1 us
    all_to_all x1, waiting for transfers between devices, local(): back = lax.all_to_all(summed, 'ep', split_axis=1, concat_axis=1, tiled=True)  7.77 us
    dot_general x1, matrix products, local(): lax.dot_general(down_mat, hidden, (((0,), (1,)), ((), ())), preferred_ele...  6.61 us
    all_to_all x1, starting transfers between devices, local(): back = lax.all_to_all(summed, 'ep', split_axis=1, concat_axis=1, tiled=True)  5.53 us
    dot_general x1, matrix products, local(): gate_pre = jnp.dot(pieces, gate_mat, preferred_element_type=jnp.float32)  3.26 us
  transfers between devices with their start and end apart: 5, of which 5 were waited for; matrix products, arithmetic and copies ran while one was open for 0% of the time, Pallas kernels for 0%

profile of v1, /device:TPU:0, one launch (start us, length us, event | category | flops | bytes accessed | tf_op | source)
XLA Modules:
  0.0 94.6 jit_solution(184464557569465970)
XLA Ops:
  6.5 0.8 copy.14
  7.3 0.1 eq.31
  7.4 0.1 fusion.51
  7.5 0.1 reduce_window_sum.11
  7.6 0.2 select_reduce_fusion
  7.8 0.1 reduce_sum.41
  8.0 0.1 convert_reduce_fusion
  8.1 1.0 %fusion.40 = f32[24]{0:T(128)S(1)} fusion(bf16[24,3072]{1,0:T(8,128)(2,1)} %param.7), kind=kLoop, calls=%fused_computation.25 | loop fusion | flops 221160 | bytes 147552 | tf_op jit(solution)/shard_map/reduce_sum | solution.py:49
  9.2 1.3 %fusion.47 = bf16[104,3072]{1,0:T(8,128)(2,1)S(1)} fusion(bf16[24,3072]{1,0:T(8,128)(2,1)} %param.7, f32[3072]{0:T(1024)} %param.8, f32[24]{0:T(128)S(1)} %add_rsqrt_fusion, s32[104,24]{0,1:T(8,128)S(1)} %convert_reduce_fusion), kind=kOutput, calls=%fused_computation.34 | convolution fusion | flops 15632832 | bytes 808800 | tf_op jit(solution)/shard_map/dot_general | solution.py:54
  10.6 15.0 %all_to_all.24 = bf16[8,13,768]{2,1,0:T(8,128)(2,1)S(1)} all-to-all(bf16[8,13,768]{2,1,0:T(8,128)(2,1)S(1)} %all_to_all.16), channel_id=1, replica_groups=mesh['ep'=8,'tp'=4] {'ep'}, dimensions={0} | all-to-all | bytes 319488 | tf_op jit(solution)/shard_map/all_to_all | solution.py:63
  25.7 4.7 %collective-permute-done = bf16[104,768]{1,0:T(8,128)(2,1)S(1)} collective-permute-done((bf16[104,768]{1,0:T(8,128)(2,1)S(1)}, bf16[104,768]{1,0:T(8,128)(2,1)S(1)}, u32[]{:S(2)}, u32[]{:S(2)}) %collective-permute-start) | collective-permute-done | bytes 159776 | tf_op jit(solution)/shard_map/ppermute | solution.py:19
  30.4 4.7 %collective-permute-done.1 = bf16[104,768]{1,0:T(8,128)(2,1)S(1)} collective-permute-done((bf16[104,768]{1,0:T(8,128)(2,1)S(1)}, bf16[104,768]{1,0:T(8,128)(2,1)S(1)}, u32[]{:S(2)}, u32[]{:S(2)}) %collective-permute-start.1) | collective-permute-done | bytes 159776 | tf_op jit(solution)/shard_map/ppermute | solution.py:19
  35.1 4.7 %collective-permute-done.2 = bf16[104,768]{1,0:T(8,128)(2,1)S(1)} collective-permute-done((bf16[104,768]{1,0:T(8,128)(2,1)S(1)}, bf16[104,768]{1,0:T(8,128)(2,1)S(1)}, u32[]{:S(2)}, u32[]{:S(2)}) %collective-permute-start.2) | collective-permute-done | bytes 159776 | tf_op jit(solution)/shard_map/ppermute | solution.py:19
  40.0 3.3 %fusion.12 = f32[104,768]{1,0:T(8,128)S(1)} fusion(bf16[1,3072,768]{2,1,0:T(8,128)(2,1)} %param.11, bf16[104,6144]{1,0:T(8,128)(2,1)S(1)} %constant_dynamic-update-slice_fusion, s32[]{:T(128)S(6)} %select_n.28), kind=kOutput, calls=%fused_computation.9 | convolution fusion | flops 490813440 | bytes 5677060 | tf_op jit(solution)/shard_map/dot_general | solution.py:65
  43.3 6.6 %fusion.9 = bf16[3072,104]{0,1:T(8,128)(2,1)} fusion(bf16[1,768,3072]{2,1,0:T(8,128)(2,1)} %param.13, f32[104,768]{1,0:T(8,128)S(1)} %fusion.12, bf16[1,3072,768]{2,1,0:T(8,128)(2,1)} %param.12, bf16[104,6144]{1,0:T(8,128)(2,1)S(1)} %constant_dynamic-update-slice_fusion, s32[]{:T(128)S(6)} %select_n.28), kind=kOutput, calls=%fused_computation.8 | convolution fusion | flops 982505472 | bytes 11034628 | tf_op jit(solution)/shard_map/dot_general | solution.py:71
  49.9 0.1 mul.80
  50.0 0.1 copy.17
  50.1 20.9 %reduce-scatter.2.cloned.1.call-done = bf16[768,104]{0,1:T(8,128)(2,1)} async-done(((bf16[3072,104]{0,1:T(8,128)(2,1)}), bf16[768,104]{0,1:T(8,128)(2,1)}) %reduce-scatter.2.cloned.1.call-update) | async-done | bytes 159760 | tf_op jit(solution)/shard_map/reduce_scatter | solution.py:70
  71.0 1.6 %all_to_all.19 = bf16[768,8,13]{0,2,1:T(8,128)(2,1)} reshape(bf16[768,104]{0,1:T(8,128)(2,1)} %reduce-scatter.2.cloned.1.call-done) | data formatting | bytes 319488 | tf_op jit(solution)/shard_map/all_to_all | solution.py:78
  72.6 5.5 %all-to-all-start.1 = ((bf16[768,8,13]{0,2,1:T(8,128)(2,1)}), bf16[768,8,13]{0,2,1:T(8,128)(2,1)S(1)}, u32[]{:S(2)}, u32[]{:S(2)}) async-start(bf16[768,8,13]{0,2,1:T(8,128)(2,1)} %all_to_all.19), calls=%async_computation.2 | async-start | bytes 393216 | tf_op jit(solution)/shard_map/all_to_all | solution.py:78
  78.2 7.8 %all-to-all-done.1 = bf16[768,8,13]{0,2,1:T(8,128)(2,1)S(1)} async-done(((bf16[768,8,13]{0,2,1:T(8,128)(2,1)}), bf16[768,8,13]{0,2,1:T(8,128)(2,1)S(1)}, u32[]{:S(2)}, u32[]{:S(2)}) %all-to-all-start.1) | async-done | bytes 159776 | tf_op jit(solution)/shard_map/all_to_all | solution.py:78
  86.0 0.8 gather_fusion
  86.8 0.1 reshape.54
  86.9 0.9 multiply_reduce_fusion
  (25 shorter events, 0.5 us)
Async XLA Ops:
  6.5 64.4 %reduce-scatter.2.cloned.1.call-start = ((), (), s32[]{:S(2)}) async-start(), calls=%async_computation.3 | async-start | bytes 798720 | tf_op jit(solution)/shard_map/reduce_scatter | solution.py:70
  25.7 4.8 %collective-permute-start = (bf16[104,768]{1,0:T(8,128)(2,1)S(1)}, bf16[104,768]{1,0:T(8,128)(2,1)S(1)}, u32[]{:S(2)}, u32[]{:S(2)}) collective-permute-start(bf16[104,768]{1,0:T(8,128)(2,1)S(1)} %all_to_all.18), channel_id=1, source_target_pairs={{0,1},{1,2},{2,3},{3,0},{4,5},{5,6},{6,7},{7,4},{8,9},{9,10},{10,1... | collective-permute-start | bytes 479240 | tf_op jit(solution)/shard_map/ppermute | solution.py:19
  30.4 4.7 %collective-permute-start.1 = (bf16[104,768]{1,0:T(8,128)(2,1)S(1)}, bf16[104,768]{1,0:T(8,128)(2,1)S(1)}, u32[]{:S(2)}, u32[]{:S(2)}) collective-permute-start(bf16[104,768]{1,0:T(8,128)(2,1)S(1)} %collective-permute-done), channel_id=1, source_target_pairs={{0,1},{1,2},{2,3},{3,0},{4,5},{5,6},{6,7},{7,4},{8,9},{9,10},{10,1... | collective-permute-start | bytes 479240 | tf_op jit(solution)/shard_map/ppermute | solution.py:19
  35.1 4.7 %collective-permute-start.2 = (bf16[104,768]{1,0:T(8,128)(2,1)S(1)}, bf16[104,768]{1,0:T(8,128)(2,1)S(1)}, u32[]{:S(2)}, u32[]{:S(2)}) collective-permute-start(bf16[104,768]{1,0:T(8,128)(2,1)S(1)} %collective-permute-done.1), channel_id=1, source_target_pairs={{0,1},{1,2},{2,3},{3,0},{4,5},{5,6},{6,7},{7,4},{8,9},{9,10},{10,1... | collective-permute-start | bytes 479240 | tf_op jit(solution)/shard_map/ppermute | solution.py:19
  43.2 6.7 %copy-start = (f32[24,4]{0,1:T(4,128)S(1)}, f32[24,4]{0,1:T(4,128)}, u32[]{:S(2)}) copy-start(f32[24,4]{0,1:T(4,128)} %param.10) | copy-start | bytes 1156
  72.6 13.3 %all-to-all-start.1 = ((bf16[768,8,13]{0,2,1:T(8,128)(2,1)}), bf16[768,8,13]{0,2,1:T(8,128)(2,1)S(1)}, u32[]{:S(2)}, u32[]{:S(2)}) async-start(bf16[768,8,13]{0,2,1:T(8,128)(2,1)} %all_to_all.19), calls=%async_computation.2 | async-start | bytes 393216 | tf_op jit(solution)/shard_map/all_to_all | solution.py:78
Sparse Core Ops, SparseCore 0:
  50.0 20.9 reduce-scatter.1
